TPU v7x, 128 devices: a whole 4x4x4 slice. The times are simulated.
128 devices in a mesh: sp: 64 (over z, y, x), tp: 2 (over core).
Axes of the slice: x: 4, y: 4, z: 4, core: 2. Of those that a mesh axis runs over, the one named last changes fastest.
Arguments:
- stream: bfloat16 [16384, 2048], P(('sp', 'tp')), may hold values from -3 to 3
- query_narrow: bfloat16 [16384, 1024], P('sp', 'tp'), may hold values from -6 to 6
- key_narrow: bfloat16 [16384, 128], P('sp', 'tp'), may hold values from -6 to 6
- value_narrow: bfloat16 [16384, 128], P('sp', 'tp'), may hold values from -6 to 6
- query_broad: bfloat16 [16384, 1024], P('sp', 'tp'), may hold values from -6 to 6
- key_broad: bfloat16 [16384, 256], P('sp', 'tp'), may hold values from -6 to 6
- value_broad: bfloat16 [16384, 256], P('sp', 'tp'), may hold values from -6 to 6
- narrow_query_gain: float32 [64], replicated, may hold values from 1.5 to 9
- narrow_key_gain: float32 [64], replicated, may hold values from 1.5 to 9
- broad_query_gain: float32 [128], replicated, may hold values from 1.5 to 9
- broad_key_gain: float32 [128], replicated, may hold values from 1.5 to 9
- out_weight: bfloat16 [2048, 2048], replicated, may hold values from -0.125 to 0.125
- norm_gain: float32 [2048], replicated, may hold values from 0.1 to 1.9
- gate_weight: bfloat16 [64, 2048, 1024], P('sp', None, 'tp'), may hold values from -0.125 to 0.125
- up_weight: bfloat16 [64, 2048, 1024], P('sp', None, 'tp'), may hold values from -0.125 to 0.125
- down_weight: bfloat16 [64, 1024, 2048], P('sp', 'tp'), may hold values from -0.1875 to 0.1875
- route_ids: int32 [16384, 2], P(('sp', 'tp')), may hold values from 0 to 63, all different within a row; in each aligned block of 128 rows (0 to 127, 128 to 255, ...) at most 8 rows name the same one
- route_weights: float32 [16384, 2], P(('sp', 'tp')), may hold values from 0.1 to 1
Outputs:
- result: bfloat16 [16384, 2048], P(('sp', 'tp'))
Inputs may be any that keep to these rules, and one draw needn't show every extreme that they name: `route_ids`: in each aligned block of 128 rows no expert is named by more than 8 rows, a bound that some block reaches.
All inputs are finite; a program needn't handle non-finite values.
Results may differ from a plain program's by a relative error of at most 0.015.
The roundings to bfloat16 on the way count: a program that leaves them out, or rounds other values in their place, can miss the bound.
Values may be sent and summed in bfloat16 or wider, within the bound.
A program may use at most 128 MiB of HBM per device.

v0:
```python
import math
import jax
import jax.numpy as jnp
from jax import lax
from jax.sharding import PartitionSpec as P

HA = 16
DA = 64
DB = 128
GRID_W = 128
eps = 1e-06
theta = 10000.0


def cut_along(value, dim, size):
    before, after = (value.shape[:dim], value.shape[dim + 1 :])
    return jnp.moveaxis(value.reshape(*before, size, -1, *after), dim, 0)


def summed_on_arrival(value, axis, dim):
    size = lax.axis_size(axis)
    blocks = lax.all_to_all(cut_along(value, dim, size), axis, 0, 0, tiled=True)
    return jnp.sum(blocks.astype(jnp.float32), axis=0)


def joined_along(blocks, dim):
    shape = list(blocks.shape[1:])
    shape[dim] *= blocks.shape[0]
    return jnp.moveaxis(blocks, 0, dim).reshape(shape)


def copy_for_each(value, axis):
    size = lax.axis_size(axis)
    return lax.all_to_all(
        jnp.broadcast_to(value[None], (size, *value.shape)), axis, 0, 0, tiled=True
    )


def gather_directly(value, axis, dim):
    return joined_along(copy_for_each(value, axis), dim)


def rotate_grid(normed, positions):
    count, heads, dim = normed.shape
    freqs = dim // 4
    inverse = theta ** (-jnp.arange(freqs, dtype=jnp.float32) / freqs)
    rows = (positions // GRID_W).astype(jnp.float32)
    cols = (positions % GRID_W).astype(jnp.float32)
    angles = jnp.stack([rows[:, None] * inverse, cols[:, None] * inverse], axis=1)
    cosine = jnp.cos(angles)[:, None]
    sine = jnp.sin(angles)[:, None]
    split = normed.reshape(count, heads, 2, 2, freqs)
    first = split[..., 0, :]
    second = split[..., 1, :]
    turned = jnp.stack([first * cosine - second * sine, second * cosine + first * sine], axis=-2)
    return turned.reshape(count, heads, dim)


def prepare(raw, gain, dim, positions):
    count = raw.shape[0]
    values = raw.astype(jnp.float32).reshape(count, -1, dim)
    scaled = values * lax.rsqrt(jnp.mean(values * values, axis=-1, keepdims=True) + eps) * gain
    return rotate_grid(scaled, positions).reshape(count, -1).astype(jnp.bfloat16)


def arrange(queries, kv_width, dim):
    rows = queries.shape[0]
    heads_kv = kv_width // dim
    shaped = queries.reshape(rows, heads_kv, -1, dim)
    groups = shaped.shape[2]
    start = (
        jnp.full((heads_kv, groups, rows), -1e30, jnp.float32),
        jnp.zeros((heads_kv, groups, rows), jnp.float32),
        jnp.zeros((heads_kv, groups, rows, dim), jnp.float32),
    )
    return (shaped, start)


def attend_block(state, queries, keys, values):
    peak, total, summed = state
    dim = queries.shape[-1]
    scores = jnp.einsum(
        "qhgd,khd->hgqk", queries, keys, preferred_element_type=jnp.float32
    ) * dim ** (-0.5)
    fresh = jnp.maximum(peak, jnp.max(scores, axis=-1))
    weights = jnp.exp(scores - fresh[..., None])
    shrink = jnp.exp(peak - fresh)
    total = total * shrink + jnp.sum(weights, axis=-1)
    summed = summed * shrink[..., None] + jnp.einsum(
        "hgqk,khd->hgqd", weights.astype(jnp.bfloat16), values, preferred_element_type=jnp.float32
    )
    return (fresh, total, summed)


def sweep(state, keys, values, queries):
    rows = keys.shape[0]
    size = math.gcd(rows, 2048)
    count = rows // size

    def step(carry, block):
        return (attend_block(carry, queries, block[0], block[1]), None)

    blocks = (
        keys.reshape(count, size, keys.shape[1], keys.shape[2]),
        values.reshape(count, size, values.shape[1], values.shape[2]),
    )
    state, _ = lax.scan(step, state, blocks)
    return state


def make_fold(shaped_n, shaped_b, state, pieces):
    keys_n, values_n, keys_b, values_b = pieces
    rows = keys_n.shape[0]
    first = sweep(state[0], keys_n.reshape(rows, -1, DA), values_n.reshape(rows, -1, DA), shaped_n)
    second = sweep(state[1], keys_b.reshape(rows, -1, DB), values_b.reshape(rows, -1, DB), shaped_b)
    return (first, second)


def finish(state):
    peak, total, summed = state
    heads_out = summed / total[..., None]
    rows = heads_out.shape[2]
    return jnp.transpose(heads_out, (2, 0, 1, 3)).reshape(rows, -1).astype(jnp.bfloat16)


def local(
    stream,
    query_narrow,
    key_narrow,
    value_narrow,
    query_broad,
    key_broad,
    value_broad,
    narrow_query_gain,
    narrow_key_gain,
    broad_query_gain,
    broad_key_gain,
    out_weight,
    norm_gain,
    gate_weight,
    up_weight,
    down_weight,
    route_ids,
    route_weights,
):
    count = query_narrow.shape[0]
    positions = lax.axis_index("sp") * count + jnp.arange(count, dtype=jnp.int32)
    queries_n = prepare(query_narrow, narrow_query_gain, DA, positions)
    keys_n = prepare(key_narrow, narrow_key_gain, DA, positions)
    queries_b = prepare(query_broad, broad_query_gain, DB, positions)
    keys_b = prepare(key_broad, broad_key_gain, DB, positions)
    shaped_n, start_n = arrange(queries_n, keys_n.shape[1], DA)
    shaped_b, start_b = arrange(queries_b, keys_b.shape[1], DB)
    state = make_fold(
        shaped_n,
        shaped_b,
        (start_n, start_b),
        (
            lax.all_gather(keys_n, "sp", axis=0, tiled=True),
            lax.all_gather(value_narrow, "sp", axis=0, tiled=True),
            lax.all_gather(keys_b, "sp", axis=0, tiled=True),
            lax.all_gather(value_broad, "sp", axis=0, tiled=True),
        ),
    )
    heads_n = finish(state[0])
    heads_b = finish(state[1])
    width = heads_n.shape[1]
    place = lax.axis_index("tp")
    local_weight = jnp.concatenate(
        [
            lax.dynamic_slice_in_dim(out_weight, place * width, width, 0),
            lax.dynamic_slice_in_dim(out_weight, HA * DA + place * width, width, 0),
        ],
        axis=0,
    )
    local_heads = jnp.concatenate([heads_n, heads_b], axis=1)
    picked = local_heads
    mixed = summed_on_arrival(
        jnp.dot(picked, local_weight, preferred_element_type=jnp.float32).astype(jnp.bfloat16),
        "tp",
        0,
    )
    wide = (stream.astype(jnp.float32) + mixed).astype(jnp.bfloat16).astype(jnp.float32)
    normed = (
        wide * lax.rsqrt(jnp.mean(wide * wide, axis=-1, keepdims=True) + eps) * norm_gain
    ).astype(jnp.bfloat16)
    tokens_here, topk = route_ids.shape
    width_model = normed.shape[1]
    experts = lax.axis_size("sp")
    capacity = (2 * tokens_here * topk + experts - 1) // experts
    flat = route_ids.reshape(-1)
    hits = (flat[:, None] == jnp.arange(experts, dtype=jnp.int32)[None, :]).astype(jnp.int32)
    ranks = jnp.sum((jnp.cumsum(hits, axis=0) - 1) * hits, axis=1)
    slots = flat * capacity + ranks
    table = (jnp.arange(experts * capacity, dtype=jnp.int32)[:, None] == slots[None, :]).astype(
        jnp.bfloat16
    )
    table = jnp.sum(table.reshape(experts * capacity, tokens_here, topk), axis=2)
    sent = jnp.dot(table, normed, preferred_element_type=jnp.float32).astype(jnp.bfloat16)
    sent = sent.reshape(experts, capacity, width_model)
    piece = gather_directly(
        lax.all_to_all(sent, "sp", split_axis=0, concat_axis=0, tiled=True), "tp", 0
    )
    rows = piece.reshape(-1, piece.shape[-1])
    gate = jnp.dot(rows, gate_weight[0], preferred_element_type=jnp.float32)
    upper = jnp.dot(rows, up_weight[0], preferred_element_type=jnp.float32)
    hidden = (jax.nn.silu(gate) * upper).astype(jnp.bfloat16)
    partial_out = jnp.dot(hidden, down_weight[0], preferred_element_type=jnp.float32).astype(
        jnp.bfloat16
    )
    terms = lax.optimization_barrier(partial_out).astype(jnp.float32).reshape(piece.shape)
    summed = summed_on_arrival(terms.astype(jnp.bfloat16), "tp", 0).astype(jnp.bfloat16)
    back = lax.all_to_all(summed, "sp", split_axis=0, concat_axis=0, tiled=True)
    picked = jnp.take(back.reshape(experts * capacity, width_model), slots, axis=0)
    picked = picked.astype(jnp.float32).reshape(tokens_here, topk, width_model)
    routed = jnp.sum(picked * route_weights[..., None], axis=1)
    return (wide + routed).astype(jnp.bfloat16)


def solution(mesh):
    return jax.shard_map(
        local,
        mesh=mesh,
        in_specs=(
            P(("sp", "tp"), None),
            P("sp", "tp"),
            P("sp", "tp"),
            P("sp", "tp"),
            P("sp", "tp"),
            P("sp", "tp"),
            P("sp", "tp"),
            P(),
            P(),
            P(),
            P(),
            P(),
            P(),
            P("sp", None, "tp"),
            P("sp", None, "tp"),
            P("sp", "tp", None),
            P(("sp", "tp"), None),
            P(("sp", "tp"), None),
        ),
        out_specs=P(("sp", "tp"), None),
        check_vma=False,
    )
```

profile of v0, /device:TPU:0, one launch (start us, length us, event | category | flops | bytes accessed | tf_op | source)
XLA Modules:
  0.0 630.0 jit_solution(12985772197260481180)
XLA Ops:
  25.9 53.0 %all-gather.5.cloned.1.call-done = bf16[16384,64]{0,1:T(8,128)(2,1)} async-done(((bf16[256,64]{0,1:T(8,128)(2,1)}), bf16[16384,64]{0,1:T(8,128)(2,1)}) %all-gather.5.cloned.1.call-update) | async-done | bytes 2097168 | tf_op jit(solution)/shard_map/all_gather | solution.py:159
  84.2 63.0 %all-gather.7.cloned.1.call-done = bf16[16384,64]{0,1:T(8,128)(2,1)} async-done(((bf16[256,64]{0,1:T(8,128)(2,1)}), bf16[16384,64]{0,1:T(8,128)(2,1)}) %all-gather.7.cloned.1.call-update) | async-done | bytes 2097168 | tf_op jit(solution)/shard_map/all_gather | solution.py:160
  152.5 219.9 %while.30 = (s32[]{:T(128)}, f32[1,8,256]{2,1,0:T(8,128)S(1)}, f32[1,8,256]{2,1,0:T(8,128)S(1)}, f32[1,8,256,64]{2,3,1,0:T(8,128)}, bf16[8,2048,1,64]{1,3,2,0:T(...) while((s32[]{:T(128)}, f32[1,8,256]{2,1,0:T(8,128)S(1)}, ...), condition=%wide.region_5.6_spmd.clone, body=%wide.region_2.5_spmd.clone.sunk | while | flops 1107701760 | bytes 52298852 | solution.py:107
  152.8 9.0 %bitcast_reduce_fusion.6 = (f32[8,256]{1,0:T(8,128)S(1)}, f32[2048,256,8]{1,0,2:T(8,128)}) fusion(bf16[256,1,8,64]{0,3,2,1:T(8,128)(2,1)S(1)} %get-tuple-element.395, bf16[8,2048,1,64]{1,3,2,0:T(8,128)(2,1)} %get-tuple-element.394, s32[]{:T(128)} %get-tuple-element.381), kind=kOutput, calls=%fused_computation.2.clone.1 | convolution fusion | flops 545257472 | bytes 17310208 | tf_op jit(solution)/shard_map/while/body/eval_jaxpr/qhgd,khd->hgqk/dot_general | solution.py:82
  161.8 9.6 %fusion.116 = f32[1,8,256,64]{2,3,1,0:T(8,128)} fusion(f32[2048,256,8]{1,0,2:T(8,128)} %get-tuple-element.332, f32[8,256]{1,0:T(8,128)S(1)} %bitcast.237, f32[1,8,256,64]{2,3,1,0:T(8,128)} %get-tuple-element.384, bf16[8,2048,1,64]{1,3,2,0:T(8,128)(2,1)} %get-tuple-element.396, s32[]{:T(128)} %get-tuple-element.381, ...), kind=kOutput, calls=%fused_computation.9.clone.1 | convolution fusion | flops 549847040 | bytes 18104832 | tf_op jit(solution)/shard_map/while/body/eval_jaxpr/hgqk,khd->hgqd/dot_general | solution.py:89
  171.5 8.6 %fusion.115 = f32[8,256]{1,0:T(8,128)S(1)} fusion(f32[2048,256,8]{1,0,2:T(8,128)} %get-tuple-element.332, f32[8,256]{1,0:T(8,128)S(1)} %bitcast.238), kind=kLoop, calls=%fused_computation.5.clone.1 | loop fusion | flops 12580864 | bytes 16793600 | tf_op jit(solution)/shard_map/while/body/eval_jaxpr/reduce_sum | solution.py:88
  180.1 9.0 %bitcast_reduce_fusion.6 = (f32[8,256]{1,0:T(8,128)S(1)}, f32[2048,256,8]{1,0,2:T(8,128)}) fusion(bf16[256,1,8,64]{0,3,2,1:T(8,128)(2,1)S(1)} %get-tuple-element.395, bf16[8,2048,1,64]{1,3,2,0:T(8,128)(2,1)} %get-tuple-element.394, s32[]{:T(128)} %get-tuple-element.381), kind=kOutput, calls=%fused_computation.2.clone.1 | convolution fusion | flops 545257472 | bytes 17310208 | tf_op jit(solution)/shard_map/while/body/eval_jaxpr/qhgd,khd->hgqk/dot_general | solution.py:82
  189.1 9.7 %fusion.116 = f32[1,8,256,64]{2,3,1,0:T(8,128)} fusion(f32[2048,256,8]{1,0,2:T(8,128)} %get-tuple-element.332, f32[8,256]{1,0:T(8,128)S(1)} %bitcast.237, f32[1,8,256,64]{2,3,1,0:T(8,128)} %get-tuple-element.384, bf16[8,2048,1,64]{1,3,2,0:T(8,128)(2,1)} %get-tuple-element.396, s32[]{:T(128)} %get-tuple-element.381, ...), kind=kOutput, calls=%fused_computation.9.clone.1 | convolution fusion | flops 549847040 | bytes 18104832 | tf_op jit(solution)/shard_map/while/body/eval_jaxpr/hgqk,khd->hgqd/dot_general | solution.py:89
  198.8 8.9 %fusion.115 = f32[8,256]{1,0:T(8,128)S(1)} fusion(f32[2048,256,8]{1,0,2:T(8,128)} %get-tuple-element.332, f32[8,256]{1,0:T(8,128)S(1)} %bitcast.238), kind=kLoop, calls=%fused_computation.5.clone.1 | loop fusion | flops 12580864 | bytes 16793600 | tf_op jit(solution)/shard_map/while/body/eval_jaxpr/reduce_sum | solution.py:88
  207.8 9.0 %bitcast_reduce_fusion.6 = (f32[8,256]{1,0:T(8,128)S(1)}, f32[2048,256,8]{1,0,2:T(8,128)}) fusion(bf16[256,1,8,64]{0,3,2,1:T(8,128)(2,1)S(1)} %get-tuple-element.395, bf16[8,2048,1,64]{1,3,2,0:T(8,128)(2,1)} %get-tuple-element.394, s32[]{:T(128)} %get-tuple-element.381), kind=kOutput, calls=%fused_computation.2.clone.1 | convolution fusion | flops 545257472 | bytes 17310208 | tf_op jit(solution)/shard_map/while/body/eval_jaxpr/qhgd,khd->hgqk/dot_general | solution.py:82
  216.8 10.0 %fusion.116 = f32[1,8,256,64]{2,3,1,0:T(8,128)} fusion(f32[2048,256,8]{1,0,2:T(8,128)} %get-tuple-element.332, f32[8,256]{1,0:T(8,128)S(1)} %bitcast.237, f32[1,8,256,64]{2,3,1,0:T(8,128)} %get-tuple-element.384, bf16[8,2048,1,64]{1,3,2,0:T(8,128)(2,1)} %get-tuple-element.396, s32[]{:T(128)} %get-tuple-element.381, ...), kind=kOutput, calls=%fused_computation.9.clone.1 | convolution fusion | flops 549847040 | bytes 18104832 | tf_op jit(solution)/shard_map/while/body/eval_jaxpr/hgqk,khd->hgqd/dot_general | solution.py:89
  226.8 8.6 %fusion.115 = f32[8,256]{1,0:T(8,128)S(1)} fusion(f32[2048,256,8]{1,0,2:T(8,128)} %get-tuple-element.332, f32[8,256]{1,0:T(8,128)S(1)} %bitcast.238), kind=kLoop, calls=%fused_computation.5.clone.1 | loop fusion | flops 12580864 | bytes 16793600 | tf_op jit(solution)/shard_map/while/body/eval_jaxpr/reduce_sum | solution.py:88
  235.4 9.0 %bitcast_reduce_fusion.6 = (f32[8,256]{1,0:T(8,128)S(1)}, f32[2048,256,8]{1,0,2:T(8,128)}) fusion(bf16[256,1,8,64]{0,3,2,1:T(8,128)(2,1)S(1)} %get-tuple-element.395, bf16[8,2048,1,64]{1,3,2,0:T(8,128)(2,1)} %get-tuple-element.394, s32[]{:T(128)} %get-tuple-element.381), kind=kOutput, calls=%fused_computation.2.clone.1 | convolution fusion | flops 545257472 | bytes 17310208 | tf_op jit(solution)/shard_map/while/body/eval_jaxpr/qhgd,khd->hgqk/dot_general | solution.py:82
  244.5 9.7 %fusion.116 = f32[1,8,256,64]{2,3,1,0:T(8,128)} fusion(f32[2048,256,8]{1,0,2:T(8,128)} %get-tuple-element.332, f32[8,256]{1,0:T(8,128)S(1)} %bitcast.237, f32[1,8,256,64]{2,3,1,0:T(8,128)} %get-tuple-element.384, bf16[8,2048,1,64]{1,3,2,0:T(8,128)(2,1)} %get-tuple-element.396, s32[]{:T(128)} %get-tuple-element.381, ...), kind=kOutput, calls=%fused_computation.9.clone.1 | convolution fusion | flops 549847040 | bytes 18104832 | tf_op jit(solution)/shard_map/while/body/eval_jaxpr/hgqk,khd->hgqd/dot_general | solution.py:89
  254.1 8.6 %fusion.115 = f32[8,256]{1,0:T(8,128)S(1)} fusion(f32[2048,256,8]{1,0,2:T(8,128)} %get-tuple-element.332, f32[8,256]{1,0:T(8,128)S(1)} %bitcast.238), kind=kLoop, calls=%fused_computation.5.clone.1 | loop fusion | flops 12580864 | bytes 16793600 | tf_op jit(solution)/shard_map/while/body/eval_jaxpr/reduce_sum | solution.py:88
  262.8 9.1 %bitcast_reduce_fusion.6 = (f32[8,256]{1,0:T(8,128)S(1)}, f32[2048,256,8]{1,0,2:T(8,128)}) fusion(bf16[256,1,8,64]{0,3,2,1:T(8,128)(2,1)S(1)} %get-tuple-element.395, bf16[8,2048,1,64]{1,3,2,0:T(8,128)(2,1)} %get-tuple-element.394, s32[]{:T(128)} %get-tuple-element.381), kind=kOutput, calls=%fused_computation.2.clone.1 | convolution fusion | flops 545257472 | bytes 17310208 | tf_op jit(solution)/shard_map/while/body/eval_jaxpr/qhgd,khd->hgqk/dot_general | solution.py:82
  271.9 9.7 %fusion.116 = f32[1,8,256,64]{2,3,1,0:T(8,128)} fusion(f32[2048,256,8]{1,0,2:T(8,128)} %get-tuple-element.332, f32[8,256]{1,0:T(8,128)S(1)} %bitcast.237, f32[1,8,256,64]{2,3,1,0:T(8,128)} %get-tuple-element.384, bf16[8,2048,1,64]{1,3,2,0:T(8,128)(2,1)} %get-tuple-element.396, s32[]{:T(128)} %get-tuple-element.381, ...), kind=kOutput, calls=%fused_computation.9.clone.1 | convolution fusion | flops 549847040 | bytes 18104832 | tf_op jit(solution)/shard_map/while/body/eval_jaxpr/hgqk,khd->hgqd/dot_general | solution.py:89
  281.5 8.9 %fusion.115 = f32[8,256]{1,0:T(8,128)S(1)} fusion(f32[2048,256,8]{1,0,2:T(8,128)} %get-tuple-element.332, f32[8,256]{1,0:T(8,128)S(1)} %bitcast.238), kind=kLoop, calls=%fused_computation.5.clone.1 | loop fusion | flops 12580864 | bytes 16793600 | tf_op jit(solution)/shard_map/while/body/eval_jaxpr/reduce_sum | solution.py:88
  290.5 9.0 %bitcast_reduce_fusion.6 = (f32[8,256]{1,0:T(8,128)S(1)}, f32[2048,256,8]{1,0,2:T(8,128)}) fusion(bf16[256,1,8,64]{0,3,2,1:T(8,128)(2,1)S(1)} %get-tuple-element.395, bf16[8,2048,1,64]{1,3,2,0:T(8,128)(2,1)} %get-tuple-element.394, s32[]{:T(128)} %get-tuple-element.381), kind=kOutput, calls=%fused_computation.2.clone.1 | convolution fusion | flops 545257472 | bytes 17310208 | tf_op jit(solution)/shard_map/while/body/eval_jaxpr/qhgd,khd->hgqk/dot_general | solution.py:82
  299.6 9.7 %fusion.116 = f32[1,8,256,64]{2,3,1,0:T(8,128)} fusion(f32[2048,256,8]{1,0,2:T(8,128)} %get-tuple-element.332, f32[8,256]{1,0:T(8,128)S(1)} %bitcast.237, f32[1,8,256,64]{2,3,1,0:T(8,128)} %get-tuple-element.384, bf16[8,2048,1,64]{1,3,2,0:T(8,128)(2,1)} %get-tuple-element.396, s32[]{:T(128)} %get-tuple-element.381, ...), kind=kOutput, calls=%fused_computation.9.clone.1 | convolution fusion | flops 549847040 | bytes 18104832 | tf_op jit(solution)/shard_map/while/body/eval_jaxpr/hgqk,khd->hgqd/dot_general | solution.py:89
  309.2 8.6 %fusion.115 = f32[8,256]{1,0:T(8,128)S(1)} fusion(f32[2048,256,8]{1,0,2:T(8,128)} %get-tuple-element.332, f32[8,256]{1,0:T(8,128)S(1)} %bitcast.238), kind=kLoop, calls=%fused_computation.5.clone.1 | loop fusion | flops 12580864 | bytes 16793600 | tf_op jit(solution)/shard_map/while/body/eval_jaxpr/reduce_sum | solution.py:88
  317.8 9.0 %bitcast_reduce_fusion.6 = (f32[8,256]{1,0:T(8,128)S(1)}, f32[2048,256,8]{1,0,2:T(8,128)}) fusion(bf16[256,1,8,64]{0,3,2,1:T(8,128)(2,1)S(1)} %get-tuple-element.395, bf16[8,2048,1,64]{1,3,2,0:T(8,128)(2,1)} %get-tuple-element.394, s32[]{:T(128)} %get-tuple-element.381), kind=kOutput, calls=%fused_computation.2.clone.1 | convolution fusion | flops 545257472 | bytes 17310208 | tf_op jit(solution)/shard_map/while/body/eval_jaxpr/qhgd,khd->hgqk/dot_general | solution.py:82
  326.9 9.7 %fusion.116 = f32[1,8,256,64]{2,3,1,0:T(8,128)} fusion(f32[2048,256,8]{1,0,2:T(8,128)} %get-tuple-element.332, f32[8,256]{1,0:T(8,128)S(1)} %bitcast.237, f32[1,8,256,64]{2,3,1,0:T(8,128)} %get-tuple-element.384, bf16[8,2048,1,64]{1,3,2,0:T(8,128)(2,1)} %get-tuple-element.396, s32[]{:T(128)} %get-tuple-element.381, ...), kind=kOutput, calls=%fused_computation.9.clone.1 | convolution fusion | flops 549847040 | bytes 18104832 | tf_op jit(solution)/shard_map/while/body/eval_jaxpr/hgqk,khd->hgqd/dot_general | solution.py:89
  336.5 8.6 %fusion.115 = f32[8,256]{1,0:T(8,128)S(1)} fusion(f32[2048,256,8]{1,0,2:T(8,128)} %get-tuple-element.332, f32[8,256]{1,0:T(8,128)S(1)} %bitcast.238), kind=kLoop, calls=%fused_computation.5.clone.1 | loop fusion | flops 12580864 | bytes 16793600 | tf_op jit(solution)/shard_map/while/body/eval_jaxpr/reduce_sum | solution.py:88
  345.1 9.0 %bitcast_reduce_fusion.6 = (f32[8,256]{1,0:T(8,128)S(1)}, f32[2048,256,8]{1,0,2:T(8,128)}) fusion(bf16[256,1,8,64]{0,3,2,1:T(8,128)(2,1)S(1)} %get-tuple-element.395, bf16[8,2048,1,64]{1,3,2,0:T(8,128)(2,1)} %get-tuple-element.394, s32[]{:T(128)} %get-tuple-element.381), kind=kOutput, calls=%fused_computation.2.clone.1 | convolution fusion | flops 545257472 | bytes 17310208 | tf_op jit(solution)/shard_map/while/body/eval_jaxpr/qhgd,khd->hgqk/dot_general | solution.py:82
  354.2 9.7 %fusion.116 = f32[1,8,256,64]{2,3,1,0:T(8,128)} fusion(f32[2048,256,8]{1,0,2:T(8,128)} %get-tuple-element.332, f32[8,256]{1,0:T(8,128)S(1)} %bitcast.237, f32[1,8,256,64]{2,3,1,0:T(8,128)} %get-tuple-element.384, bf16[8,2048,1,64]{1,3,2,0:T(8,128)(2,1)} %get-tuple-element.396, s32[]{:T(128)} %get-tuple-element.381, ...), kind=kOutput, calls=%fused_computation.9.clone.1 | convolution fusion | flops 549847040 | bytes 18104832 | tf_op jit(solution)/shard_map/while/body/eval_jaxpr/hgqk,khd->hgqd/dot_general | solution.py:89
  363.8 8.6 %fusion.115 = f32[8,256]{1,0:T(8,128)S(1)} fusion(f32[2048,256,8]{1,0,2:T(8,128)} %get-tuple-element.332, f32[8,256]{1,0:T(8,128)S(1)} %bitcast.238), kind=kLoop, calls=%fused_computation.5.clone.1 | loop fusion | flops 12580864 | bytes 16793600 | tf_op jit(solution)/shard_map/while/body/eval_jaxpr/reduce_sum | solution.py:88
  374.2 6.3 %copy.79 = bf16[16384,128]{1,0:T(8,128)(2,1)} copy(bf16[16384,128]{0,1:T(8,128)(2,1)} %all-gather.9.cloned.1.call-done) | data formatting | bytes 8388608
  380.6 103.4 %while.31 = (s32[]{:T(128)}, f32[1,4,256]{2,1,0:T(4,128)S(1)}, f32[1,4,256]{2,1,0:T(4,128)S(1)}, f32[1,4,256,128]{3,2,1,0:T(8,128)S(1)}, bf16[8,2048,1,128]{3,1,...) while((s32[]{:T(128)}, f32[1,4,256]{2,1,0:T(4,128)S(1)}, ...), condition=%wide.region_11.12_spmd.clone, body=%wide.region_8.11_spmd.clone.sunk | while | flops 1090918400 | bytes 61146240 | solution.py:107
  381.1 5.5 bitcast_reduce_fusion.7
  386.6 5.3 fusion.121
  393.9 5.5 bitcast_reduce_fusion.7
  406.8 5.5 bitcast_reduce_fusion.7
  412.3 5.3 fusion.121
  419.7 5.5 bitcast_reduce_fusion.7
  425.2 5.3 fusion.121
  432.5 5.5 bitcast_reduce_fusion.7
  445.4 5.5 bitcast_reduce_fusion.7
  458.3 5.5 bitcast_reduce_fusion.7
  471.1 5.5 bitcast_reduce_fusion.7
  476.7 5.3 fusion.121
  493.8 38.3 %all_to_all.26 = bf16[64,8,2048]{2,1,0:T(8,128)(2,1)S(1)} all-to-all(bf16[64,8,2048]{2,1,0:T(8,128)(2,1)S(1)} %fusion.48), channel_id=1, replica_groups=mesh['sp'=64,'tp'=2] {'sp'}, dimensions={0} | all-to-all | bytes 4194304 | tf_op jit(solution)/shard_map/all_to_all | solution.py:202
  532.7 7.4 %all_to_all.27 = bf16[2,64,8,2048]{3,2,1,0:T(8,128)(2,1)S(1)} all-to-all(bf16[2,64,8,2048]{3,2,1,0:T(8,128)(2,1)S(1)} %broadcast_in_dim.28), channel_id=1, replica_groups=mesh['sp'=64,'tp'=2] {'tp'}, dimensions={0} | all-to-all | bytes 8388608 | tf_op jit(solution)/shard_map/all_to_all | solution.py:34
  545.8 10.0 %convolution_convert_fusion = bf16[1024,2048]{1,0:T(8,128)(2,1)} fusion(bf16[1,512,2048]{2,1,0:T(8,128)(2,1)S(1)} %copy-done, f32[1024,512]{1,0:T(8,128)} %fusion.53, bf16[1024,2048]{1,0:T(8,128)(2,1)} %bitcast.240, bf16[1,2048,512]{2,1,0:T(8,128)(2,1)} %param.35), kind=kOutput, calls=%fused_computation.53 | convolution fusion | flops 4300210176 | bytes 14680064 | tf_op jit(solution)/shard_map/dot_general | solution.py:208
  555.8 11.9 %all_to_all.28 = bf16[2,64,8,2048]{3,2,1,0:T(8,128)(2,1)} all-to-all(bf16[2,64,8,2048]{3,2,1,0:T(8,128)(2,1)} %bitcast.241), channel_id=1, replica_groups=mesh['sp'=64,'tp'=2] {'tp'}, dimensions={0} | all-to-all | bytes 8388608 | tf_op jit(solution)/shard_map/all_to_all | solution.py:22
  572.7 6.2 all-to-all-start.4
  579.5 29.6 %all-to-all-done.4 = bf16[64,8,2048]{2,1,0:T(8,128)(2,1)} async-done(((bf16[64,8,2048]{2,1,0:T(8,128)(2,1)}), bf16[64,8,2048]{2,1,0:T(8,128)(2,1)}, u32[]{:S(2)}, u32[]{:S(2)}) %all-to-all-start.4) | async-done | bytes 2097184 | tf_op jit(solution)/shard_map/all_to_all | solution.py:213
  616.9 5.5 multiply_reduce_fusion
  (187 shorter events, 99.4 us)
Async XLA Ops:
  6.5 539.2 %copy-start = (bf16[1,512,2048]{2,1,0:T(8,128)(2,1)S(1)}, bf16[1,512,2048]{2,1,0:T(8,128)(2,1)}, u32[]{:S(2)}) copy-start(bf16[1,512,2048]{2,1,0:T(8,128)(2,1)} %param.37) | copy-start | bytes 6291460
  6.5 13.6 %copy-start.6 = (s32[128,2]{0,1:T(2,128)S(1)}, s32[128,2]{0,1:T(2,128)}, u32[]{:S(2)}) copy-start(s32[128,2]{0,1:T(2,128)} %param.38) | copy-start | bytes 3076
  6.5 72.4 %all-gather.5.cloned.1.call-start = ((), (), s32[]{:S(2)}) async-start(), calls=%async_computation.5 | async-start | bytes 2129920 | tf_op jit(solution)/shard_map/all_gather | solution.py:159
  9.2 138.0 %all-gather.7.cloned.1.call-start = ((), (), s32[]{:S(2)}) async-start(), calls=%async_computation.6 | async-start | bytes 2129920 | tf_op jit(solution)/shard_map/all_gather | solution.py:160
  9.9 364.3 %all-gather.9.cloned.1.call-start = ((), (), s32[]{:S(2)}) async-start(), calls=%async_computation.7 | async-start | bytes 4259840 | tf_op jit(solution)/shard_map/all_gather | solution.py:161
  12.7 367.8 %all-gather.11.cloned.1.call-start = ((), (), s32[]{:S(2)}) async-start(), calls=%async_computation.8 | async-start | bytes 4259840 | tf_op jit(solution)/shard_map/all_gather | solution.py:162
  19.9 0.8 copy-start.4
  386.6 5.9 copy-start.1
  399.5 5.9 copy-start.1
  412.3 5.9 copy-start.1
  425.2 5.9 copy-start.1
  438.1 5.9 copy-start.1
  450.9 5.9 copy-start.1
  463.8 5.9 copy-start.1
  476.7 5.9 copy-start.1
  487.8 4.9 copy-start.3
  487.8 5.2 copy-start.8
  532.7 9.4 %copy-start.11 = (bf16[1,2048,512]{2,1,0:T(8,128)(2,1)S(1)}, bf16[1,2048,512]{2,1,0:T(8,128)(2,1)}, u32[]{:S(2)}) copy-start(bf16[1,2048,512]{2,1,0:T(8,128)(2,1)} %param.36) | copy-start | bytes 6291460
  540.1 2.0 copy-start.2
  567.7 11.3 %copy-start.7 = (s32[128,2]{0,1:T(2,128)S(1)}, s32[128,2]{0,1:T(2,128)}, u32[]{:S(2)}) copy-start(s32[128,2]{0,1:T(2,128)} %param.38) | copy-start | bytes 3076
  567.7 11.5 %copy-start.9 = (pred[128,2]{0,1:T(4,128)(4,1)S(1)}, pred[128,2]{0,1:T(4,128)(4,1)}, u32[]{:S(2)}) copy-start(pred[128,2]{0,1:T(4,128)(4,1)} %get-tuple-element.207) | copy-start | bytes 772
  567.7 11.7 %copy-start.10 = (f32[128,2]{0,1:T(2,128)S(1)}, f32[128,2]{0,1:T(2,128)}, u32[]{:S(2)}) copy-start(f32[128,2]{0,1:T(2,128)} %param.39) | copy-start | bytes 3076
  567.7 11.8 %copy-start.5 = (s32[256]{0:T(256)S(1)}, s32[256]{0:T(256)}, u32[]{:S(2)}) copy-start(s32[256]{0:T(256)} %copy-done.4) | copy-start | bytes 3076
  572.7 36.4 %all-to-all-start.4 = ((bf16[64,8,2048]{2,1,0:T(8,128)(2,1)}), bf16[64,8,2048]{2,1,0:T(8,128)(2,1)}, u32[]{:S(2)}, u32[]{:S(2)}) async-start(bf16[64,8,2048]{2,1,0:T(8,128)(2,1)} %reduce_sum.131), calls=%async_computation.4 | async-start | bytes 4194304 | tf_op jit(solution)/shard_map/all_to_all | solution.py:213
Sparse Core Ops, SparseCore 0:
  10.0 68.8 all-gather.4
  81.6 65.5 all-gather.6
  149.9 73.9 all-gather.8
  226.7 69.3 all-gather.10
where the time goes:
time: 638 us; the launch traced here: 630 us
  matrix products  254 us (40%)
  waiting for transfers between devices  147 us (23%)
  other arithmetic  101 us (16%)
  blocking collectives  62.3 us (10%)
  local copies, waits for them, and re-layouts  44.2 us (7%)
  between operations  13.7 us (2%)
    dot_general x16, matrix products, attend_block(): jnp.einsum('hgqk,khd->hgqd', weights.astype(jnp.bfloat16), values, prefer...  120 us
    dot_general x16, matrix products, attend_block(): jnp.einsum('qhgd,khd->hgqk', queries, keys, preferred_element_type=jnp.fl...  116 us
    reduce_sum x16, other arithmetic, attend_block(): total = total * shrink + jnp.sum(weights, axis=-1)  80.2 us
    all_gather x1, waiting for transfers between devices, local(): lax.all_gather(value_narrow, 'sp', axis=0, tiled=True)  63 us
    all_gather x1, waiting for transfers between devices, local(): lax.all_gather(keys_n, 'sp', axis=0, tiled=True)  53 us
    all_to_all x1, blocking collectives, local(): lax.all_to_all(sent, 'sp', split_axis=0, concat_axis=0, tiled=True)  38.3 us
    all_to_all x1, waiting for transfers between devices, local(): back = lax.all_to_all(summed, 'sp', split_axis=0, concat_axis=0, tiled=True)  29.6 us
    unnamed x33, local copies, waits for them, and re-layouts  23.1 us
  transfers between devices with their start and end apart: 5, of which 3 were waited for; matrix products, arithmetic and copies ran while one was open for 40% of the time, Pallas kernels for 0%

commit v1 on v0

--- a/solution.py
+++ b/solution.py
@@ -151,12 +151,19 @@
     keys_b = prepare(key_broad, broad_key_gain, DB, positions)
     shaped_n, start_n = arrange(queries_n, keys_n.shape[1], DA)
     shaped_b, start_b = arrange(queries_b, keys_b.shape[1], DB)
+
+    def _recast_lane(arr, dim_i):
+        val = lax.axis_size("sp")
+        mid_arr = jnp.stack(val * [arr], axis=0)
+        x_next = lax.all_to_all(mid_arr, axis_name="sp", split_axis=0, concat_axis=0)
+        return jnp.concatenate(x_next, axis=dim_i)
+
     state = make_fold(
         shaped_n,
         shaped_b,
         (start_n, start_b),
         (
-            lax.all_gather(keys_n, "sp", axis=0, tiled=True),
+            _recast_lane(keys_n, dim_i=0),
             lax.all_gather(value_narrow, "sp", axis=0, tiled=True),
             lax.all_gather(keys_b, "sp", axis=0, tiled=True),
             lax.all_gather(value_broad, "sp", axis=0, tiled=True),

time: 638 us -> 588 us (0.922)
  waiting for transfers between devices: 147 us -> 72.7 us
  starting transfers between devices: 6.3 us -> 18 us
  local copies, waits for them, and re-layouts: 44.2 us -> 51.7 us
    all_gather x1 -> x0, waiting for transfers between devices: 53 us -> none  [local(): lax.all_gather(keys_n, 'sp', axis=0, tiled=True)]
    all_gather x1, waiting for transfers between devices: 63 us -> 26.3 us  [local(): lax.all_gather(value_narrow, 'sp', axis=0, tiled=True)]
    all_to_all x0 -> x1, waiting for transfers between devices: none -> 15.3 us  [_recast_lane(): lax.all_to_all(mid_arr, axis_name='sp', split_axis=0, concat_axis=0)]
    all_to_all x0 -> x1, starting transfers between devices: none -> 11.8 us  [_recast_lane(): lax.all_to_all(mid_arr, axis_name='sp', split_axis=0, concat_axis=0)]
    unnamed x33 -> x36, local copies, waits for them, and re-layouts: 23.1 us -> 20.3 us
  transfers between devices with their start and end apart: 5 -> 5, of which waited for: 3 -> 3; matrix products, arithmetic and copies ran while one was open for 40% -> 46% of each run, Pallas kernels for 0% -> 0%
where the time goes in v1:
time: 588 us; the launch traced here: 578 us
  matrix products  254 us (43%)
  other arithmetic  104 us (18%)
  waiting for transfers between devices  72.7 us (12%)
  blocking collectives  62.2 us (11%)
  local copies, waits for them, and re-layouts  51.7 us (9%)
  starting transfers between devices  18 us (3%)
  between operations  13.8 us (2%)
    dot_general x16, matrix products, attend_block(): jnp.einsum('hgqk,khd->hgqd', weights.astype(jnp.bfloat16), values, prefer...  120 us
    dot_general x16, matrix products, attend_block(): jnp.einsum('qhgd,khd->hgqk', queries, keys, preferred_element_type=jnp.fl...  116 us
    reduce_sum x16, other arithmetic, attend_block(): total = total * shrink + jnp.sum(weights, axis=-1)  80.2 us
    all_to_all x1, blocking collectives, local(): lax.all_to_all(sent, 'sp', split_axis=0, concat_axis=0, tiled=True)  38.3 us
    all_to_all x1, waiting for transfers between devices, local(): back = lax.all_to_all(summed, 'sp', split_axis=0, concat_axis=0, tiled=True)  29.6 us
    all_gather x1, waiting for transfers between devices, local(): lax.all_gather(value_narrow, 'sp', axis=0, tiled=True)  26.3 us
    unnamed x36, local copies, waits for them, and re-layouts  20.3 us
    all_to_all x2, blocking collectives, summed_on_arrival(): blocks = lax.all_to_all(cut_along(value, dim, size), axis, 0, 0, tiled=True)  16.6 us
  transfers between devices with their start and end apart: 5, of which 3 were waited for; matrix products, arithmetic and copies ran while one was open for 46% of the time, Pallas kernels for 0%

profile of v1, /device:TPU:0, one launch (start us, length us, event | category | flops | bytes accessed | tf_op | source)
XLA Modules:
  0.0 578.2 jit_solution(6420926640544396844)
XLA Ops:
  14.7 11.8 %all-to-all-start = ((bf16[64,256,64]{1,2,0:T(8,128)(2,1)}), bf16[64,256,64]{1,2,0:T(8,128)(2,1)}, u32[]{:S(2)}, u32[]{:S(2)}) async-start(bf16[64,256,64]{1,2,0:T(8,128)(2,1)} %stack.34), calls=%async_computation | async-start | bytes 4194304 | tf_op jit(solution)/shard_map/all_to_all | solution.py:158
  41.4 15.3 %all-to-all-done = bf16[64,256,64]{1,2,0:T(8,128)(2,1)} async-done(((bf16[64,256,64]{1,2,0:T(8,128)(2,1)}), bf16[64,256,64]{1,2,0:T(8,128)(2,1)}, u32[]{:S(2)}, u32[]{:S(2)}) %all-to-all-start) | async-done | bytes 2097184 | tf_op jit(solution)/shard_map/all_to_all | solution.py:158
  69.1 26.3 %all-gather.4.cloned.1.call-done = bf16[16384,64]{0,1:T(8,128)(2,1)} async-done(((bf16[256,64]{0,1:T(8,128)(2,1)}), bf16[16384,64]{0,1:T(8,128)(2,1)}) %all-gather.4.cloned.1.call-update) | async-done | bytes 2097168 | tf_op jit(solution)/shard_map/all_gather | solution.py:167
  100.7 219.9 %while.30 = (s32[]{:T(128)}, f32[1,8,256]{2,1,0:T(8,128)S(1)}, f32[1,8,256]{2,1,0:T(8,128)S(1)}, f32[1,8,256,64]{2,3,1,0:T(8,128)}, bf16[8,2048,1,64]{1,3,2,0:T(...) while((s32[]{:T(128)}, f32[1,8,256]{2,1,0:T(8,128)S(1)}, ...), condition=%wide.region_5.6_spmd.clone, body=%wide.region_2.5_spmd.clone.sunk | while | flops 1107701760 | bytes 52298852 | solution.py:107
  101.0 9.0 %bitcast_reduce_fusion.6 = (f32[8,256]{1,0:T(8,128)S(1)}, f32[2048,256,8]{1,0,2:T(8,128)}) fusion(bf16[256,1,8,64]{0,3,2,1:T(8,128)(2,1)S(1)} %get-tuple-element.409, bf16[8,2048,1,64]{1,3,2,0:T(8,128)(2,1)} %get-tuple-element.408, s32[]{:T(128)} %get-tuple-element.395), kind=kOutput, calls=%fused_computation.2.clone.1 | convolution fusion | flops 545257472 | bytes 17310208 | tf_op jit(solution)/shard_map/while/body/eval_jaxpr/qhgd,khd->hgqk/dot_general | solution.py:82
  110.0 9.6 %fusion.116 = f32[1,8,256,64]{2,3,1,0:T(8,128)} fusion(f32[2048,256,8]{1,0,2:T(8,128)} %get-tuple-element.346, f32[8,256]{1,0:T(8,128)S(1)} %bitcast.233, f32[1,8,256,64]{2,3,1,0:T(8,128)} %get-tuple-element.398, bf16[8,2048,1,64]{1,3,2,0:T(8,128)(2,1)} %get-tuple-element.410, s32[]{:T(128)} %get-tuple-element.395, ...), kind=kOutput, calls=%fused_computation.9.clone.1 | convolution fusion | flops 549847040 | bytes 18104832 | tf_op jit(solution)/shard_map/while/body/eval_jaxpr/hgqk,khd->hgqd/dot_general | solution.py:89
  119.7 8.6 %fusion.115 = f32[8,256]{1,0:T(8,128)S(1)} fusion(f32[2048,256,8]{1,0,2:T(8,128)} %get-tuple-element.346, f32[8,256]{1,0:T(8,128)S(1)} %bitcast.234), kind=kLoop, calls=%fused_computation.5.clone.1 | loop fusion | flops 12580864 | bytes 16793600 | tf_op jit(solution)/shard_map/while/body/eval_jaxpr/reduce_sum | solution.py:88
  128.3 9.0 %bitcast_reduce_fusion.6 = (f32[8,256]{1,0:T(8,128)S(1)}, f32[2048,256,8]{1,0,2:T(8,128)}) fusion(bf16[256,1,8,64]{0,3,2,1:T(8,128)(2,1)S(1)} %get-tuple-element.409, bf16[8,2048,1,64]{1,3,2,0:T(8,128)(2,1)} %get-tuple-element.408, s32[]{:T(128)} %get-tuple-element.395), kind=kOutput, calls=%fused_computation.2.clone.1 | convolution fusion | flops 545257472 | bytes 17310208 | tf_op jit(solution)/shard_map/while/body/eval_jaxpr/qhgd,khd->hgqk/dot_general | solution.py:82
  137.3 9.7 %fusion.116 = f32[1,8,256,64]{2,3,1,0:T(8,128)} fusion(f32[2048,256,8]{1,0,2:T(8,128)} %get-tuple-element.346, f32[8,256]{1,0:T(8,128)S(1)} %bitcast.233, f32[1,8,256,64]{2,3,1,0:T(8,128)} %get-tuple-element.398, bf16[8,2048,1,64]{1,3,2,0:T(8,128)(2,1)} %get-tuple-element.410, s32[]{:T(128)} %get-tuple-element.395, ...), kind=kOutput, calls=%fused_computation.9.clone.1 | convolution fusion | flops 549847040 | bytes 18104832 | tf_op jit(solution)/shard_map/while/body/eval_jaxpr/hgqk,khd->hgqd/dot_general | solution.py:89
  147.0 8.9 %fusion.115 = f32[8,256]{1,0:T(8,128)S(1)} fusion(f32[2048,256,8]{1,0,2:T(8,128)} %get-tuple-element.346, f32[8,256]{1,0:T(8,128)S(1)} %bitcast.234), kind=kLoop, calls=%fused_computation.5.clone.1 | loop fusion | flops 12580864 | bytes 16793600 | tf_op jit(solution)/shard_map/while/body/eval_jaxpr/reduce_sum | solution.py:88
  156.0 9.0 %bitcast_reduce_fusion.6 = (f32[8,256]{1,0:T(8,128)S(1)}, f32[2048,256,8]{1,0,2:T(8,128)}) fusion(bf16[256,1,8,64]{0,3,2,1:T(8,128)(2,1)S(1)} %get-tuple-element.409, bf16[8,2048,1,64]{1,3,2,0:T(8,128)(2,1)} %get-tuple-element.408, s32[]{:T(128)} %get-tuple-element.395), kind=kOutput, calls=%fused_computation.2.clone.1 | convolution fusion | flops 545257472 | bytes 17310208 | tf_op jit(solution)/shard_map/while/body/eval_jaxpr/qhgd,khd->hgqk/dot_general | solution.py:82
  165.0 10.0 %fusion.116 = f32[1,8,256,64]{2,3,1,0:T(8,128)} fusion(f32[2048,256,8]{1,0,2:T(8,128)} %get-tuple-element.346, f32[8,256]{1,0:T(8,128)S(1)} %bitcast.233, f32[1,8,256,64]{2,3,1,0:T(8,128)} %get-tuple-element.398, bf16[8,2048,1,64]{1,3,2,0:T(8,128)(2,1)} %get-tuple-element.410, s32[]{:T(128)} %get-tuple-element.395, ...), kind=kOutput, calls=%fused_computation.9.clone.1 | convolution fusion | flops 549847040 | bytes 18104832 | tf_op jit(solution)/shard_map/while/body/eval_jaxpr/hgqk,khd->hgqd/dot_general | solution.py:89
  175.0 8.6 %fusion.115 = f32[8,256]{1,0:T(8,128)S(1)} fusion(f32[2048,256,8]{1,0,2:T(8,128)} %get-tuple-element.346, f32[8,256]{1,0:T(8,128)S(1)} %bitcast.234), kind=kLoop, calls=%fused_computation.5.clone.1 | loop fusion | flops 12580864 | bytes 16793600 | tf_op jit(solution)/shard_map/while/body/eval_jaxpr/reduce_sum | solution.py:88
  183.6 9.0 %bitcast_reduce_fusion.6 = (f32[8,256]{1,0:T(8,128)S(1)}, f32[2048,256,8]{1,0,2:T(8,128)}) fusion(bf16[256,1,8,64]{0,3,2,1:T(8,128)(2,1)S(1)} %get-tuple-element.409, bf16[8,2048,1,64]{1,3,2,0:T(8,128)(2,1)} %get-tuple-element.408, s32[]{:T(128)} %get-tuple-element.395), kind=kOutput, calls=%fused_computation.2.clone.1 | convolution fusion | flops 545257472 | bytes 17310208 | tf_op jit(solution)/shard_map/while/body/eval_jaxpr/qhgd,khd->hgqk/dot_general | solution.py:82
  192.7 9.7 %fusion.116 = f32[1,8,256,64]{2,3,1,0:T(8,128)} fusion(f32[2048,256,8]{1,0,2:T(8,128)} %get-tuple-element.346, f32[8,256]{1,0:T(8,128)S(1)} %bitcast.233, f32[1,8,256,64]{2,3,1,0:T(8,128)} %get-tuple-element.398, bf16[8,2048,1,64]{1,3,2,0:T(8,128)(2,1)} %get-tuple-element.410, s32[]{:T(128)} %get-tuple-element.395, ...), kind=kOutput, calls=%fused_computation.9.clone.1 | convolution fusion | flops 549847040 | bytes 18104832 | tf_op jit(solution)/shard_map/while/body/eval_jaxpr/hgqk,khd->hgqd/dot_general | solution.py:89
  202.3 8.6 %fusion.115 = f32[8,256]{1,0:T(8,128)S(1)} fusion(f32[2048,256,8]{1,0,2:T(8,128)} %get-tuple-element.346, f32[8,256]{1,0:T(8,128)S(1)} %bitcast.234), kind=kLoop, calls=%fused_computation.5.clone.1 | loop fusion | flops 12580864 | bytes 16793600 | tf_op jit(solution)/shard_map/while/body/eval_jaxpr/reduce_sum | solution.py:88
  211.0 9.1 %bitcast_reduce_fusion.6 = (f32[8,256]{1,0:T(8,128)S(1)}, f32[2048,256,8]{1,0,2:T(8,128)}) fusion(bf16[256,1,8,64]{0,3,2,1:T(8,128)(2,1)S(1)} %get-tuple-element.409, bf16[8,2048,1,64]{1,3,2,0:T(8,128)(2,1)} %get-tuple-element.408, s32[]{:T(128)} %get-tuple-element.395), kind=kOutput, calls=%fused_computation.2.clone.1 | convolution fusion | flops 545257472 | bytes 17310208 | tf_op jit(solution)/shard_map/while/body/eval_jaxpr/qhgd,khd->hgqk/dot_general | solution.py:82
  220.1 9.7 %fusion.116 = f32[1,8,256,64]{2,3,1,0:T(8,128)} fusion(f32[2048,256,8]{1,0,2:T(8,128)} %get-tuple-element.346, f32[8,256]{1,0:T(8,128)S(1)} %bitcast.233, f32[1,8,256,64]{2,3,1,0:T(8,128)} %get-tuple-element.398, bf16[8,2048,1,64]{1,3,2,0:T(8,128)(2,1)} %get-tuple-element.410, s32[]{:T(128)} %get-tuple-element.395, ...), kind=kOutput, calls=%fused_computation.9.clone.1 | convolution fusion | flops 549847040 | bytes 18104832 | tf_op jit(solution)/shard_map/while/body/eval_jaxpr/hgqk,khd->hgqd/dot_general | solution.py:89
  229.7 8.9 %fusion.115 = f32[8,256]{1,0:T(8,128)S(1)} fusion(f32[2048,256,8]{1,0,2:T(8,128)} %get-tuple-element.346, f32[8,256]{1,0:T(8,128)S(1)} %bitcast.234), kind=kLoop, calls=%fused_computation.5.clone.1 | loop fusion | flops 12580864 | bytes 16793600 | tf_op jit(solution)/shard_map/while/body/eval_jaxpr/reduce_sum | solution.py:88
  238.7 9.0 %bitcast_reduce_fusion.6 = (f32[8,256]{1,0:T(8,128)S(1)}, f32[2048,256,8]{1,0,2:T(8,128)}) fusion(bf16[256,1,8,64]{0,3,2,1:T(8,128)(2,1)S(1)} %get-tuple-element.409, bf16[8,2048,1,64]{1,3,2,0:T(8,128)(2,1)} %get-tuple-element.408, s32[]{:T(128)} %get-tuple-element.395), kind=kOutput, calls=%fused_computation.2.clone.1 | convolution fusion | flops 545257472 | bytes 17310208 | tf_op jit(solution)/shard_map/while/body/eval_jaxpr/qhgd,khd->hgqk/dot_general | solution.py:82
  247.8 9.7 %fusion.116 = f32[1,8,256,64]{2,3,1,0:T(8,128)} fusion(f32[2048,256,8]{1,0,2:T(8,128)} %get-tuple-element.346, f32[8,256]{1,0:T(8,128)S(1)} %bitcast.233, f32[1,8,256,64]{2,3,1,0:T(8,128)} %get-tuple-element.398, bf16[8,2048,1,64]{1,3,2,0:T(8,128)(2,1)} %get-tuple-element.410, s32[]{:T(128)} %get-tuple-element.395, ...), kind=kOutput, calls=%fused_computation.9.clone.1 | convolution fusion | flops 549847040 | bytes 18104832 | tf_op jit(solution)/shard_map/while/body/eval_jaxpr/hgqk,khd->hgqd/dot_general | solution.py:89
  257.4 8.6 %fusion.115 = f32[8,256]{1,0:T(8,128)S(1)} fusion(f32[2048,256,8]{1,0,2:T(8,128)} %get-tuple-element.346, f32[8,256]{1,0:T(8,128)S(1)} %bitcast.234), kind=kLoop, calls=%fused_computation.5.clone.1 | loop fusion | flops 12580864 | bytes 16793600 | tf_op jit(solution)/shard_map/while/body/eval_jaxpr/reduce_sum | solution.py:88
  266.0 9.0 %bitcast_reduce_fusion.6 = (f32[8,256]{1,0:T(8,128)S(1)}, f32[2048,256,8]{1,0,2:T(8,128)}) fusion(bf16[256,1,8,64]{0,3,2,1:T(8,128)(2,1)S(1)} %get-tuple-element.409, bf16[8,2048,1,64]{1,3,2,0:T(8,128)(2,1)} %get-tuple-element.408, s32[]{:T(128)} %get-tuple-element.395), kind=kOutput, calls=%fused_computation.2.clone.1 | convolution fusion | flops 545257472 | bytes 17310208 | tf_op jit(solution)/shard_map/while/body/eval_jaxpr/qhgd,khd->hgqk/dot_general | solution.py:82
  275.1 9.7 %fusion.116 = f32[1,8,256,64]{2,3,1,0:T(8,128)} fusion(f32[2048,256,8]{1,0,2:T(8,128)} %get-tuple-element.346, f32[8,256]{1,0:T(8,128)S(1)} %bitcast.233, f32[1,8,256,64]{2,3,1,0:T(8,128)} %get-tuple-element.398, bf16[8,2048,1,64]{1,3,2,0:T(8,128)(2,1)} %get-tuple-element.410, s32[]{:T(128)} %get-tuple-element.395, ...), kind=kOutput, calls=%fused_computation.9.clone.1 | convolution fusion | flops 549847040 | bytes 18104832 | tf_op jit(solution)/shard_map/while/body/eval_jaxpr/hgqk,khd->hgqd/dot_general | solution.py:89
  284.7 8.6 %fusion.115 = f32[8,256]{1,0:T(8,128)S(1)} fusion(f32[2048,256,8]{1,0,2:T(8,128)} %get-tuple-element.346, f32[8,256]{1,0:T(8,128)S(1)} %bitcast.234), kind=kLoop, calls=%fused_computation.5.clone.1 | loop fusion | flops 12580864 | bytes 16793600 | tf_op jit(solution)/shard_map/while/body/eval_jaxpr/reduce_sum | solution.py:88
  293.3 9.0 %bitcast_reduce_fusion.6 = (f32[8,256]{1,0:T(8,128)S(1)}, f32[2048,256,8]{1,0,2:T(8,128)}) fusion(bf16[256,1,8,64]{0,3,2,1:T(8,128)(2,1)S(1)} %get-tuple-element.409, bf16[8,2048,1,64]{1,3,2,0:T(8,128)(2,1)} %get-tuple-element.408, s32[]{:T(128)} %get-tuple-element.395), kind=kOutput, calls=%fused_computation.2.clone.1 | convolution fusion | flops 545257472 | bytes 17310208 | tf_op jit(solution)/shard_map/while/body/eval_jaxpr/qhgd,khd->hgqk/dot_general | solution.py:82
  302.4 9.7 %fusion.116 = f32[1,8,256,64]{2,3,1,0:T(8,128)} fusion(f32[2048,256,8]{1,0,2:T(8,128)} %get-tuple-element.346, f32[8,256]{1,0:T(8,128)S(1)} %bitcast.233, f32[1,8,256,64]{2,3,1,0:T(8,128)} %get-tuple-element.398, bf16[8,2048,1,64]{1,3,2,0:T(8,128)(2,1)} %get-tuple-element.410, s32[]{:T(128)} %get-tuple-element.395, ...), kind=kOutput, calls=%fused_computation.9.clone.1 | convolution fusion | flops 549847040 | bytes 18104832 | tf_op jit(solution)/shard_map/while/body/eval_jaxpr/hgqk,khd->hgqd/dot_general | solution.py:89
  312.0 8.6 %fusion.115 = f32[8,256]{1,0:T(8,128)S(1)} fusion(f32[2048,256,8]{1,0,2:T(8,128)} %get-tuple-element.346, f32[8,256]{1,0:T(8,128)S(1)} %bitcast.234), kind=kLoop, calls=%fused_computation.5.clone.1 | loop fusion | flops 12580864 | bytes 16793600 | tf_op jit(solution)/shard_map/while/body/eval_jaxpr/reduce_sum | solution.py:88
  322.4 6.3 %copy.98 = bf16[16384,128]{1,0:T(8,128)(2,1)} copy(bf16[16384,128]{0,1:T(8,128)(2,1)} %all-gather.6.cloned.1.call-done) | data formatting | bytes 8388608
  328.8 103.4 %while.31 = (s32[]{:T(128)}, f32[1,4,256]{2,1,0:T(4,128)S(1)}, f32[1,4,256]{2,1,0:T(4,128)S(1)}, f32[1,4,256,128]{3,2,1,0:T(8,128)S(1)}, bf16[8,2048,1,128]{3,1,...) while((s32[]{:T(128)}, f32[1,4,256]{2,1,0:T(4,128)S(1)}, ...), condition=%wide.region_11.12_spmd.clone, body=%wide.region_8.11_spmd.clone.sunk | while | flops 1090918400 | bytes 61146240 | solution.py:107
  329.3 5.5 bitcast_reduce_fusion.7
  342.1 5.5 bitcast_reduce_fusion.7
  347.7 5.3 fusion.121
  355.0 5.5 bitcast_reduce_fusion.7
  360.5 5.3 fusion.121
  367.9 5.5 bitcast_reduce_fusion.7
  380.7 5.5 bitcast_reduce_fusion.7
  393.6 5.5 bitcast_reduce_fusion.7
  406.5 5.5 bitcast_reduce_fusion.7
  419.3 5.5 bitcast_reduce_fusion.7
  424.9 5.3 fusion.121
  442.0 38.3 %all_to_all.31 = bf16[64,8,2048]{2,1,0:T(8,128)(2,1)S(1)} all-to-all(bf16[64,8,2048]{2,1,0:T(8,128)(2,1)S(1)} %fusion.48), channel_id=1, replica_groups=mesh['sp'=64,'tp'=2] {'sp'}, dimensions={0} | all-to-all | bytes 4194304 | tf_op jit(solution)/shard_map/all_to_all | solution.py:209
  480.9 7.4 %all_to_all.32 = bf16[2,64,8,2048]{3,2,1,0:T(8,128)(2,1)S(1)} all-to-all(bf16[2,64,8,2048]{3,2,1,0:T(8,128)(2,1)S(1)} %broadcast_in_dim.28), channel_id=1, replica_groups=mesh['sp'=64,'tp'=2] {'tp'}, dimensions={0} | all-to-all | bytes 8388608 | tf_op jit(solution)/shard_map/all_to_all | solution.py:34
  493.9 10.1 %convolution_convert_fusion = bf16[1024,2048]{1,0:T(8,128)(2,1)} fusion(bf16[1,512,2048]{2,1,0:T(8,128)(2,1)S(1)} %copy-done, f32[1024,512]{1,0:T(8,128)} %fusion.53, bf16[1024,2048]{1,0:T(8,128)(2,1)} %bitcast.236, bf16[1,2048,512]{2,1,0:T(8,128)(2,1)} %param.35), kind=kOutput, calls=%fused_computation.53 | convolution fusion | flops 4300210176 | bytes 14680064 | tf_op jit(solution)/shard_map/dot_general | solution.py:215
  504.0 11.9 %all_to_all.33 = bf16[2,64,8,2048]{3,2,1,0:T(8,128)(2,1)} all-to-all(bf16[2,64,8,2048]{3,2,1,0:T(8,128)(2,1)} %bitcast.237), channel_id=1, replica_groups=mesh['sp'=64,'tp'=2] {'tp'}, dimensions={0} | all-to-all | bytes 8388608 | tf_op jit(solution)/shard_map/all_to_all | solution.py:22
  520.9 6.2 %all-to-all-start.5 = ((bf16[64,8,2048]{2,1,0:T(8,128)(2,1)}), bf16[64,8,2048]{2,1,0:T(8,128)(2,1)}, u32[]{:S(2)}, u32[]{:S(2)}) async-start(bf16[64,8,2048]{2,1,0:T(8,128)(2,1)} %reduce_sum.131), calls=%async_computation.5 | async-start | bytes 4194304 | tf_op jit(solution)/shard_map/all_to_all | solution.py:220
  527.7 29.6 %all-to-all-done.5 = bf16[64,8,2048]{2,1,0:T(8,128)(2,1)} async-done(((bf16[64,8,2048]{2,1,0:T(8,128)(2,1)}), bf16[64,8,2048]{2,1,0:T(8,128)(2,1)}, u32[]{:S(2)}, u32[]{:S(2)}) %all-to-all-start.5) | async-done | bytes 2097184 | tf_op jit(solution)/shard_map/all_to_all | solution.py:220
  565.1 5.5 multiply_reduce_fusion
  (192 shorter events, 115.4 us)
Async XLA Ops:
  6.5 487.4 %copy-start = (bf16[1,512,2048]{2,1,0:T(8,128)(2,1)S(1)}, bf16[1,512,2048]{2,1,0:T(8,128)(2,1)}, u32[]{:S(2)}) copy-start(bf16[1,512,2048]{2,1,0:T(8,128)(2,1)} %param.37) | copy-start | bytes 6291460
  6.5 20.8 %copy-start.7 = (s32[128,2]{0,1:T(2,128)S(1)}, s32[128,2]{0,1:T(2,128)}, u32[]{:S(2)}) copy-start(s32[128,2]{0,1:T(2,128)} %param.38) | copy-start | bytes 3076
  6.5 22.3 %copy-start.4 = (bf16[256,512]{1,0:T(8,128)(2,1)S(1)}, bf16[256,512]{1,0:T(8,128)(2,1)}, u32[]{:S(2)}) copy-start(bf16[256,512]{1,0:T(8,128)(2,1)} %param.23) | copy-start | bytes 786436
  6.5 88.9 %all-gather.4.cloned.1.call-start = ((), (), s32[]{:S(2)}) async-start(), calls=%async_computation.6 | async-start | bytes 2129920 | tf_op jit(solution)/shard_map/all_gather | solution.py:167
  7.3 315.2 %all-gather.6.cloned.1.call-start = ((), (), s32[]{:S(2)}) async-start(), calls=%async_computation.7 | async-start | bytes 4259840 | tf_op jit(solution)/shard_map/all_gather | solution.py:168
  8.3 20.6 %copy-start.12 = (f32[64]{0:T(128)S(1)}, f32[64]{0:T(128)}, u32[]{:S(2)}) copy-start(f32[64]{0:T(128)} %param.29) | copy-start | bytes 772
  14.7 42.0 %all-to-all-start = ((bf16[64,256,64]{1,2,0:T(8,128)(2,1)}), bf16[64,256,64]{1,2,0:T(8,128)(2,1)}, u32[]{:S(2)}, u32[]{:S(2)}) async-start(bf16[64,256,64]{1,2,0:T(8,128)(2,1)} %stack.34), calls=%async_computation | async-start | bytes 4194304 | tf_op jit(solution)/shard_map/all_to_all | solution.py:158
  26.5 302.2 %all-gather.8.cloned.1.call-start = ((), (), s32[]{:S(2)}) async-start(), calls=%async_computation.8 | async-start | bytes 4259840 | tf_op jit(solution)/shard_map/all_gather | solution.py:169
  34.6 6.8 %copy-start.5 = (s32[256]{0:T(256)}, s32[256]{0:T(256)S(1)}, u32[]{:S(2)}) copy-start(s32[256]{0:T(256)S(1)} %fusion.78) | copy-start | bytes 3076
  334.8 5.9 %copy-start.1 = (f32[2048,256,4]{1,0,2:T(8,128)S(1)}, f32[2048,256,4]{1,0,2:T(8,128)}, u32[]{:S(2)}) copy-start(f32[2048,256,4]{1,0,2:T(8,128)} %get-tuple-element.357) | copy-start | bytes 25165828 | tf_op jit(solution)/shard_map/while
  347.7 5.9 %copy-start.1 = (f32[2048,256,4]{1,0,2:T(8,128)S(1)}, f32[2048,256,4]{1,0,2:T(8,128)}, u32[]{:S(2)}) copy-start(f32[2048,256,4]{1,0,2:T(8,128)} %get-tuple-element.357) | copy-start | bytes 25165828 | tf_op jit(solution)/shard_map/while
  360.5 5.9 %copy-start.1 = (f32[2048,256,4]{1,0,2:T(8,128)S(1)}, f32[2048,256,4]{1,0,2:T(8,128)}, u32[]{:S(2)}) copy-start(f32[2048,256,4]{1,0,2:T(8,128)} %get-tuple-element.357) | copy-start | bytes 25165828 | tf_op jit(solution)/shard_map/while
  373.4 5.9 %copy-start.1 = (f32[2048,256,4]{1,0,2:T(8,128)S(1)}, f32[2048,256,4]{1,0,2:T(8,128)}, u32[]{:S(2)}) copy-start(f32[2048,256,4]{1,0,2:T(8,128)} %get-tuple-element.357) | copy-start | bytes 25165828 | tf_op jit(solution)/shard_map/while
  386.3 5.9 %copy-start.1 = (f32[2048,256,4]{1,0,2:T(8,128)S(1)}, f32[2048,256,4]{1,0,2:T(8,128)}, u32[]{:S(2)}) copy-start(f32[2048,256,4]{1,0,2:T(8,128)} %get-tuple-element.357) | copy-start | bytes 25165828 | tf_op jit(solution)/shard_map/while
  399.1 5.9 %copy-start.1 = (f32[2048,256,4]{1,0,2:T(8,128)S(1)}, f32[2048,256,4]{1,0,2:T(8,128)}, u32[]{:S(2)}) copy-start(f32[2048,256,4]{1,0,2:T(8,128)} %get-tuple-element.357) | copy-start | bytes 25165828 | tf_op jit(solution)/shard_map/while
  412.0 5.9 %copy-start.1 = (f32[2048,256,4]{1,0,2:T(8,128)S(1)}, f32[2048,256,4]{1,0,2:T(8,128)}, u32[]{:S(2)}) copy-start(f32[2048,256,4]{1,0,2:T(8,128)} %get-tuple-element.357) | copy-start | bytes 25165828 | tf_op jit(solution)/shard_map/while
  424.9 5.9 %copy-start.1 = (f32[2048,256,4]{1,0,2:T(8,128)S(1)}, f32[2048,256,4]{1,0,2:T(8,128)}, u32[]{:S(2)}) copy-start(f32[2048,256,4]{1,0,2:T(8,128)} %get-tuple-element.357) | copy-start | bytes 25165828 | tf_op jit(solution)/shard_map/while
  436.0 4.9 copy-start.3
  436.1 5.2 copy-start.9
  480.9 9.4 %copy-start.13 = (bf16[1,2048,512]{2,1,0:T(8,128)(2,1)S(1)}, bf16[1,2048,512]{2,1,0:T(8,128)(2,1)}, u32[]{:S(2)}) copy-start(bf16[1,2048,512]{2,1,0:T(8,128)(2,1)} %param.36) | copy-start | bytes 6291460
  488.3 2.0 copy-start.2
  515.9 11.3 %copy-start.8 = (s32[128,2]{0,1:T(2,128)S(1)}, s32[128,2]{0,1:T(2,128)}, u32[]{:S(2)}) copy-start(s32[128,2]{0,1:T(2,128)} %param.38) | copy-start | bytes 3076
  515.9 11.5 %copy-start.10 = (pred[128,2]{0,1:T(4,128)(4,1)S(1)}, pred[128,2]{0,1:T(4,128)(4,1)}, u32[]{:S(2)}) copy-start(pred[128,2]{0,1:T(4,128)(4,1)} %get-tuple-element.221) | copy-start | bytes 772
  515.9 11.7 %copy-start.11 = (f32[128,2]{0,1:T(2,128)S(1)}, f32[128,2]{0,1:T(2,128)}, u32[]{:S(2)}) copy-start(f32[128,2]{0,1:T(2,128)} %param.39) | copy-start | bytes 3076
  515.9 11.8 %copy-start.6 = (s32[256]{0:T(256)S(1)}, s32[256]{0:T(256)}, u32[]{:S(2)}) copy-start(s32[256]{0:T(256)} %copy-done.5) | copy-start | bytes 3076
  520.9 36.4 %all-to-all-start.5 = ((bf16[64,8,2048]{2,1,0:T(8,128)(2,1)}), bf16[64,8,2048]{2,1,0:T(8,128)(2,1)}, u32[]{:S(2)}, u32[]{:S(2)}) async-start(bf16[64,8,2048]{2,1,0:T(8,128)(2,1)} %reduce_sum.131), calls=%async_computation.5 | async-start | bytes 4194304 | tf_op jit(solution)/shard_map/all_to_all | solution.py:220
Sparse Core Ops, SparseCore 0:
  10.0 85.3 all-gather.3
  98.1 73.9 all-gather.5
  175.1 69.3 all-gather.7
